TPU v7x, 32 devices: a whole 2x2x4 slice. The times are simulated.
32 devices in a mesh: sp: 8 (over z, y), tp: 4 (over x, core).
Axes of the slice: x: 2, y: 2, z: 4, core: 2. Of those that a mesh axis runs over, the one named last changes fastest.
Arguments:
- tokens: bfloat16 [2048, 4096], P('sp'), may hold values from -6 to 6
- norm_gain: float32 [4096], replicated, may hold values from 0.1 to 1.9
- w_query: bfloat16 [4096, 512], P('sp', 'tp'), may hold values from -0.09375 to 0.09375
- w_key: bfloat16 [4096, 512], P('sp', 'tp'), may hold values from -0.09375 to 0.09375
- w_value: bfloat16 [4096, 1024], P('sp', 'tp'), may hold values from -0.09375 to 0.09375
- w_gates: bfloat16 [4096, 2, 2, 4], P(None, None, None, 'tp'), may hold values from -0.09375 to 0.09375
- input_bias: float32 [2, 4], P(None, 'tp'), may hold values from -2 to 90
- forget_bias: float32 [2, 4], P(None, 'tp'), as said below
- decay_shift: float32 [2, 2048, 4], P(None, 'sp', 'tp'), may hold values from -2.5 to 0
- head_gain: float32 [1024], P('tp'), may hold values from 0.1 to 1.9
- w_conv_b: bfloat16 [4096, 1024], P('sp', 'tp'), may hold values from -0.09375 to 0.09375
- w_conv_c: bfloat16 [4096, 1024], P('sp', 'tp'), may hold values from -0.09375 to 0.09375
- w_conv_in: bfloat16 [4096, 1024], P('sp', 'tp'), may hold values from -0.09375 to 0.09375
- conv_taps: bfloat16 [3, 1024], P(None, 'tp'), may hold values from -3.5 to 3.5
- w_out: bfloat16 [2048, 4096], P('sp', 'tp'), may hold values from -0.125 to 0.125
Outputs:
- mixed_out: bfloat16 [2048, 4096], P('sp', 'tp')
Inputs may be any that keep to these rules, and one draw needn't show every extreme that they name: `forget_bias`: at most the natural logarithm of 2048 plus 2.
All inputs are finite; a program needn't handle non-finite values.
Results may differ from a plain program's by a relative error of at most 0.02.
Values may be sent and summed in bfloat16 or wider, within the bound.
A program may use at most 128 MiB of HBM per device.

v0:
```python
import jax
import jax.numpy as jnp
from jax import lax
from jax.sharding import PartitionSpec as P

DQK = 128
DV = 256
BLOCK = 128
EPS = 1e-06
HIGH = lax.Precision.HIGHEST
LOWEST = -1e30


def carried_in(value, axis, join, neutral, backward):
    count, mine = (lax.axis_size(axis), lax.axis_index(axis))
    pieces = jax.tree.map(lambda part: lax.all_gather(part, axis), value)
    if backward:
        pieces = jax.tree.map(lambda part: part[::-1], pieces)
        mine = count - 1 - mine
    subtotal = jax.tree.map(
        lambda part, zero: jnp.full_like(part, 0) + jnp.asarray(zero, part.dtype), value, neutral
    )

    def lap(position, subtotal):
        longer = join(subtotal, jax.tree.map(lambda part: part[position], pieces))
        return jax.tree.map(lambda new, old: jnp.where(position < mine, new, old), longer, subtotal)

    return lax.fori_loop(0, count - 1, lap, subtotal)


def padded_2(value, sides, width):
    for axis, dim in sides:
        size, length = (lax.axis_size(axis), value.shape[dim])
        up = [(i, (i + 1) % size) for i in range(size - 1)]
        down = [(j, i) for i, j in up]
        last = lax.slice_in_dim(value, length - width, length, axis=dim)
        initial = lax.slice_in_dim(value, 0, width, axis=dim)
        before = lax.ppermute(last, axis, up)
        after = lax.ppermute(initial, axis, down)
        value = jnp.concatenate([before, value, after], axis=dim)
    return value


def row_norm(tokens, norm_gain):
    values = tokens.astype(jnp.float32)
    inverse_rms = lax.rsqrt(jnp.mean(values * values, axis=-1, keepdims=True) + EPS)
    return (values * inverse_rms * norm_gain).astype(jnp.bfloat16)


def to_heads(source, head_count):
    length = source.shape[0]
    return source.astype(jnp.float32).reshape(length, head_count, -1).transpose(1, 0, 2)


def combine(earlier, later):
    total_a, memory_a, normer_a, stable_a = earlier
    total_b, memory_b, normer_b, stable_b = later
    stable = jnp.maximum(stable_a + total_b, stable_b)
    weight_a = jnp.exp(stable_a + total_b - stable)
    weight_b = jnp.exp(stable_b - stable)
    memory = weight_a[..., None, None] * memory_a + weight_b[..., None, None] * memory_b
    normer = weight_a[..., None] * normer_a + weight_b[..., None] * normer_b
    return (total_a + total_b, memory, normer, stable)


def local_pass(queries, keys_all, values_all, in_gate, log_forget, backward):
    head_count, length = in_gate.shape
    block_count = length // BLOCK

    def blocked(source):
        return source.reshape((head_count, block_count, BLOCK) + source.shape[2:])

    query_block = blocked(queries)
    key_blk = blocked(keys_all)
    value_blk = blocked(values_all)
    gate_blk = blocked(in_gate)
    cumulative = jnp.cumsum(blocked(log_forget), axis=-1)
    block_total = cumulative[..., -1]
    log_update = block_total[..., None] - cumulative + gate_blk
    block_stable = jnp.max(log_update, axis=-1)
    update = jnp.exp(log_update - block_stable[..., None])
    block_memory = jnp.einsum(
        "hcsv,hcsd->hcvd", value_blk * update[..., None], key_blk, precision=HIGH
    )
    block_normer = jnp.einsum("hcs,hcsd->hcd", update, key_blk, precision=HIGH)
    identity = (
        jnp.zeros((head_count,), jnp.float32),
        jnp.zeros((head_count, DV, DQK), jnp.float32),
        jnp.zeros((head_count, DQK), jnp.float32),
        jnp.full((head_count,), LOWEST, jnp.float32),
    )
    running = identity
    prefixes = []
    for index in range(block_count):
        prefixes.append(running)
        running = combine(
            running,
            (
                block_total[:, index],
                block_memory[:, index],
                block_normer[:, index],
                block_stable[:, index],
            ),
        )
    if backward:
        incoming = carried_in(running, "sp", combine, identity, True)
    else:
        incoming = carried_in(running, "sp", combine, identity, False)
    stacked = tuple((jnp.stack(members, axis=1) for members in zip(*prefixes)))
    expanded = tuple((member[:, None] for member in incoming))
    ignored, start_memory, start_normer, start_stable = combine(expanded, stacked)
    lower_mask = jnp.tril(jnp.ones((BLOCK, BLOCK), dtype=bool))
    log_weight = jnp.where(
        lower_mask,
        cumulative[..., :, None] - cumulative[..., None, :] + gate_blk[..., None, :],
        -jnp.inf,
    )
    carried = cumulative + start_stable[..., None]
    running_max = jnp.maximum(carried, jnp.max(log_weight, axis=-1))
    scores = jnp.einsum("hctd,hcsd->hcts", query_block, key_blk, precision=HIGH) * jnp.exp(
        log_weight - running_max[..., None]
    )
    carry_weight = jnp.exp(carried - running_max)
    numerator = jnp.einsum("hcts,hcsv->hctv", scores, value_blk, precision=HIGH) + carry_weight[
        ..., None
    ] * jnp.einsum("hcvd,hctd->hctv", start_memory, query_block, precision=HIGH)
    denominator = jnp.sum(scores, axis=-1) + carry_weight * jnp.einsum(
        "hcd,hctd->hct", start_normer, query_block, precision=HIGH
    )
    result = numerator / jnp.maximum(jnp.abs(denominator), jnp.exp(-running_max))[..., None]
    return result.reshape(head_count, length, DV)


def flipped(source):
    return jnp.flip(source, axis=1)


def lstm_branch(
    normed,
    query_proj,
    key_proj,
    value_proj,
    w_gates,
    input_bias,
    forget_bias,
    decay_shift,
    head_gain,
):
    length = normed.shape[0]
    head_count = w_gates.shape[-1]
    gate_pre = jnp.dot(
        normed,
        w_gates.reshape(w_gates.shape[0], 4 * head_count),
        preferred_element_type=jnp.float32,
    ).reshape(length, 2, 2, head_count)
    queries = to_heads(query_proj, head_count) * DQK ** (-0.5)
    keys_all = to_heads(key_proj, head_count)
    values_all = to_heads(value_proj, head_count)
    summed = jnp.zeros((head_count, length, DV), jnp.float32)
    for direction in range(2):
        in_gate = (gate_pre[:, direction, 0, :] + input_bias[direction]).T
        log_forget = (
            jax.nn.log_sigmoid(gate_pre[:, direction, 1, :] + forget_bias[direction])
            + decay_shift[direction]
        ).T
        if direction == 1:
            result = flipped(
                local_pass(
                    flipped(queries),
                    flipped(keys_all),
                    flipped(values_all),
                    flipped(in_gate),
                    flipped(log_forget),
                    True,
                )
            )
        else:
            result = local_pass(queries, keys_all, values_all, in_gate, log_forget, False)
        summed = summed + result
    inverse_rms = lax.rsqrt(jnp.mean(summed * summed, axis=-1, keepdims=True) + EPS)
    return ((summed * inverse_rms).transpose(1, 0, 2) * head_gain.reshape(head_count, DV)).astype(
        jnp.bfloat16
    )


def conv_branch(gate_outer, gate_inner, conv_input, conv_taps):
    length = gate_outer.shape[0]
    mixed_in = (gate_inner.astype(jnp.float32) * conv_input.astype(jnp.float32)).astype(
        jnp.bfloat16
    )
    padded = padded_2(mixed_in, (("sp", 0),), 1).astype(jnp.float32)
    taps_wide = conv_taps.astype(jnp.float32)
    filtered = taps_wide[0] * padded[:-2] + taps_wide[1] * padded[1:-1] + taps_wide[2] * padded[2:]
    return (gate_outer.astype(jnp.float32) * filtered).astype(jnp.bfloat16).reshape(length, -1, DV)


def projected(normed, matrices):
    return tuple(
        (
            jnp.dot(normed, matrix, preferred_element_type=jnp.float32).astype(jnp.bfloat16)
            for matrix in matrices
        )
    )


def body(
    tokens,
    norm_gain,
    w_query,
    w_key,
    w_value,
    w_gates,
    input_bias,
    forget_bias,
    decay_shift,
    head_gain,
    w_conv_b,
    w_conv_c,
    w_conv_in,
    conv_taps,
    w_out,
):
    normed = row_norm(tokens, norm_gain)
    length = normed.shape[0]
    whole_mats = (
        lax.all_gather(w_query, "sp", axis=0, tiled=True),
        lax.all_gather(w_key, "sp", axis=0, tiled=True),
        lax.all_gather(w_value, "sp", axis=0, tiled=True),
        lax.all_gather(w_conv_b, "sp", axis=0, tiled=True),
        lax.all_gather(w_conv_c, "sp", axis=0, tiled=True),
        lax.all_gather(w_conv_in, "sp", axis=0, tiled=True),
    )
    query_proj, key_proj, value_proj, gate_outer, gate_inner, conv_input = projected(
        normed, whole_mats
    )
    lstm_out = lstm_branch(
        normed,
        query_proj,
        key_proj,
        value_proj,
        w_gates,
        input_bias,
        forget_bias,
        decay_shift,
        head_gain,
    )
    conv_out = conv_branch(gate_outer, gate_inner, conv_input, conv_taps)
    joined = jnp.stack([lstm_out, conv_out], axis=2).reshape(length, -1)
    joined_all = lax.all_gather(joined, "tp", axis=1, tiled=True)
    out_whole = lax.all_gather(w_out, "sp", axis=0, tiled=True)
    return jnp.dot(joined_all, out_whole, preferred_element_type=jnp.float32).astype(jnp.bfloat16)


def solution(mesh):
    placed = (
        P("sp", None),
        P(),
        P("sp", "tp"),
        P("sp", "tp"),
        P("sp", "tp"),
        P(None, None, None, "tp"),
        P(None, "tp"),
        P(None, "tp"),
        P(None, "sp", "tp"),
        P("tp"),
        P("sp", "tp"),
        P("sp", "tp"),
        P("sp", "tp"),
        P(None, "tp"),
        P("sp", "tp"),
    )
    return jax.shard_map(body, mesh=mesh, in_specs=placed, out_specs=P("sp", "tp"), check_vma=False)
```

profile of v0, /device:TPU:0, one launch (start us, length us, event | category | flops | bytes accessed | tf_op | source)
XLA Modules:
  0.0 511.0 jit_solution(5849541648931565221)
XLA Ops:
  10.6 2.1 fusion.8
  13.9 2.2 fusion.10
  16.8 1.4 fusion.62
  20.9 1.9 fusion.66
  23.6 3.6 fusion.84
  27.1 1.3 dynamic-update-slice.1
  29.5 1.9 fusion.65
  32.9 3.7 fusion.87
  36.6 1.3 dynamic-update-slice.3
  37.9 23.7 %all-reduce.8 = (f32[8]{0:T(128)}, f32[8]{0:T(128)}, f32[8]{0:T(128)S(1)}, f32[8]{0:T(128)S(1)}) all-reduce(f32[8]{0:T(128)S(1)} %fusion.66, f32[8]{0:T(128)S(1)} %dynamic-update-slice.1, f32[8]{0:T(128)S(1)} %fusion.65, f32[8]{0:T(128)S(1)} %dynamic-update-slice.3), channel_id=2, replica_groups=mesh['sp'=8,'tp'=4] {'sp'}, use_global_device_ids=true, to_apply=%add.4 | all-reduce | flops 32 | bytes 256
  63.0 1.7 fusion.85
  68.6 1.8 fusion.88
  74.7 0.8 select_reduce_fusion
  76.3 1.9 convolution_convert_fusion.5
  78.7 15.1 %all-gather.15.cloned.1.call-done = bf16[4096,128]{1,0:T(8,128)(2,1)} async-done(((bf16[512,128]{1,0:T(8,128)(2,1)}), bf16[4096,128]{1,0:T(8,128)(2,1)}) %all-gather.15.cloned.1.call-update) | async-done | bytes 1048592 | tf_op jit(solution)/shard_map/all_gather | solution.py:226
  93.8 2.6 broadcast_multiply_fusion.1
  96.4 47.4 %all-gather.19.cloned.1.call-done = bf16[4096,256]{1,0:T(8,128)(2,1)} async-done(((bf16[512,256]{1,0:T(8,128)(2,1)}), bf16[4096,256]{1,0:T(8,128)(2,1)}) %all-gather.19.cloned.1.call-update) | async-done | bytes 2097168 | tf_op jit(solution)/shard_map/all_gather | solution.py:228
  143.8 2.3 fusion.83
  147.8 18.2 %all_gather.78 = f32[8,1,128]{2,1,0:T(1,128)S(1)} all-gather(f32[1,1,128]{2,1,0:T(1,128)S(1)} %get-tuple-element.431), channel_id=1, replica_groups=mesh['sp'=8,'tp'=4] {'sp'}, dimensions={0}, use_global_device_ids=true | all-gather | bytes 4608 | tf_op jit(solution)/shard_map/all_gather | solution.py:16
  167.1 17.2 %all_gather.72 = f32[8,1,128]{2,1,0:T(1,128)} all-gather(f32[1,1,128]{2,1,0:T(1,128)S(1)} %get-tuple-element.439), channel_id=1, replica_groups=mesh['sp'=8,'tp'=4] {'sp'}, dimensions={0}, use_global_device_ids=true | all-gather | bytes 4608 | tf_op jit(solution)/shard_map/all_gather | solution.py:16
  184.5 9.1 %all-gather.27.cloned.1.call-done = bf16[4096,256]{1,0:T(8,128)(2,1)} async-done(((bf16[512,256]{1,0:T(8,128)(2,1)}), bf16[4096,256]{1,0:T(8,128)(2,1)}) %all-gather.27.cloned.1.call-update) | async-done | bytes 2097168 | tf_op jit(solution)/shard_map/all_gather | solution.py:230
  193.7 2.5 fusion.20
  196.2 47.1 %all-gather.29.cloned.1.call-done = bf16[4096,256]{1,0:T(8,128)(2,1)} async-done(((bf16[512,256]{1,0:T(8,128)(2,1)}), bf16[4096,256]{1,0:T(8,128)(2,1)}) %all-gather.29.cloned.1.call-update) | async-done | bytes 2097168 | tf_op jit(solution)/shard_map/all_gather | solution.py:231
  243.3 2.5 fusion.19
  245.9 2.5 collective-permute-start
  248.4 1.3 collective-permute-start.1
  252.0 3.9 collective-permute-done.1
  255.9 1.0 maximum_convert_fusion
  256.9 36.2 %all-gather.25.cloned.1.call-done = bf16[4096,256]{1,0:T(8,128)(2,1)} async-done(((bf16[512,256]{1,0:T(8,128)(2,1)}), bf16[4096,256]{1,0:T(8,128)(2,1)}) %all-gather.25.cloned.1.call-update) | async-done | bytes 2097168 | tf_op jit(solution)/shard_map/all_gather | solution.py:229
  293.1 3.3 fusion.24
  296.3 37.7 %all-gather.21.cloned.1.call-done = f32[8,1,256,128]{3,2,1,0:T(8,128)} async-done(((f32[1,1,256,128]{3,2,1,0:T(8,128)}), f32[8,1,256,128]{3,2,1,0:T(8,128)}) %all-gather.21.cloned.1.call-update) | async-done | bytes 1048592 | tf_op jit(solution)/shard_map/all_gather | solution.py:16
  334.1 29.4 %while.36 = (s32[]{:T(128)}, f32[1,256,128]{2,1,0:T(8,128)S(1)}, f32[1,128]{1,0:T(1,128)S(1)}, f32[1]{0:T(128)}, s32[]{:T(128)}, /*index=5*/f32[8,1]{0,1:T(1,128...) while((s32[]{:T(128)}, f32[1,256,128]{2,1,0:T(8,128)S(1)}, ...), condition=%wide.region_4.5_spmd.clone, body=%wide.region_3.4_spmd.clone.sunk | while | flops 164489 | bytes 395004 | solution.py:28
  336.6 1.0 fusion.133
  340.8 1.0 fusion.133
  345.0 1.0 fusion.133
  349.2 1.0 fusion.133
  353.3 1.0 fusion.133
  357.5 1.0 fusion.133
  361.8 1.0 fusion.133
  363.5 11.7 %all-gather.23.cloned.1.call-done = f32[8,1,256,128]{3,2,1,0:T(8,128)} async-done(((f32[1,1,256,128]{3,2,1,0:T(8,128)}), f32[8,1,256,128]{3,2,1,0:T(8,128)}) %all-gather.23.cloned.1.call-update) | async-done | bytes 1048592 | tf_op jit(solution)/shard_map/all_gather | solution.py:16
  375.2 1.3 rev.34
  376.6 23.4 %while.37 = (s32[]{:T(128)}, f32[1,256,128]{2,1,0:T(8,128)S(1)}, f32[1,128]{1,0:T(1,128)S(1)}, f32[1]{0:T(128)}, s32[]{:T(128)}, /*index=5*/f32[8,1]{0,1:T(1,128...) while((s32[]{:T(128)}, f32[1,256,128]{2,1,0:T(8,128)S(1)}, ...), condition=%wide.region_10.11_spmd.clone, body=%wide.region_9.10_spmd.clone.sunk | while | flops 164489 | bytes 395004 | solution.py:28
  400.0 1.3 subtract_exponential_fusion.7
  401.3 1.4 subtract_exponential_fusion.5
  402.7 1.4 subtract_exponential_fusion.4
  409.9 15.0 %all-gather.31.cloned.1.call-done = bf16[256,2048]{0,1:T(8,128)(2,1)} async-done(((bf16[256,512]{0,1:T(8,128)(2,1)}), bf16[256,2048]{0,1:T(8,128)(2,1)}) %all-gather.31.cloned.1.call-update) | async-done | bytes 1048592 | tf_op jit(solution)/shard_map/all_gather | solution.py:249
  424.8 74.8 %all-gather.33.cloned.1.call-done = bf16[2048,1024]{1,0:T(8,128)(2,1)} async-done(((bf16[256,1024]{1,0:T(8,128)(2,1)}), bf16[2048,1024]{1,0:T(8,128)(2,1)}) %all-gather.33.cloned.1.call-update) | async-done | bytes 4194320 | tf_op jit(solution)/shard_map/all_gather | solution.py:250
  499.6 4.6 convolution_convert_fusion
  (197 shorter events, 43.8 us)
Async XLA Ops:
  6.5 6.1 %copy-start.11 = (bf16[4096,2,2,1]{0,2,3,1:T(2,128)(2,1)S(1)}, bf16[4096,2,2,1]{0,2,3,1:T(2,128)(2,1)}, u32[]{:S(2)}) copy-start(bf16[4096,2,2,1]{0,2,3,1:T(2,128)(2,1)} %param.24) | copy-start | bytes 98308
  6.5 6.2 %copy-start.27 = (f32[2,1]{0,1:T(1,128)S(1)}, f32[2,1]{0,1:T(1,128)}, u32[]{:S(2)}) copy-start(f32[2,1]{0,1:T(1,128)} %param.26) | copy-start | bytes 28
  6.5 6.8 %copy-start.28 = (f32[2,1]{0,1:T(1,128)S(1)}, f32[2,1]{0,1:T(1,128)}, u32[]{:S(2)}) copy-start(f32[2,1]{0,1:T(1,128)} %param.25) | copy-start | bytes 28
  6.5 7.4 %copy-start.16 = (f32[4096]{0:T(1024)S(1)}, f32[4096]{0:T(1024)}, u32[]{:S(2)}) copy-start(f32[4096]{0:T(1024)} %param.20) | copy-start | bytes 49156
  6.5 69.7 %all-gather.17.cloned.1.call-start = ((), (), s32[]{:S(2)}) async-start(), calls=%async_computation.1 | async-start | bytes 1179648 | tf_op jit(solution)/shard_map/all_gather | solution.py:227
  7.3 86.5 %all-gather.15.cloned.1.call-start = ((), (), s32[]{:S(2)}) async-start(), calls=%async_computation | async-start | bytes 1179648 | tf_op jit(solution)/shard_map/all_gather | solution.py:226
  8.0 135.7 %all-gather.19.cloned.1.call-start = ((), (), s32[]{:S(2)}) async-start(), calls=%async_computation.2 | async-start | bytes 2359296 | tf_op jit(solution)/shard_map/all_gather | solution.py:228
  8.8 184.9 %all-gather.27.cloned.1.call-start = ((), (), s32[]{:S(2)}) async-start(), calls=%async_computation.6 | async-start | bytes 2359296 | tf_op jit(solution)/shard_map/all_gather | solution.py:230
  9.3 233.9 %all-gather.29.cloned.1.call-start = ((), (), s32[]{:S(2)}) async-start(), calls=%async_computation.7 | async-start | bytes 2359296 | tf_op jit(solution)/shard_map/all_gather | solution.py:231
  9.9 283.2 %all-gather.25.cloned.1.call-start = ((), (), s32[]{:S(2)}) async-start(), calls=%async_computation.5 | async-start | bytes 2359296 | tf_op jit(solution)/shard_map/all_gather | solution.py:229
  10.5 323.5 %all-gather.21.cloned.1.call-start = ((), (), s32[]{:S(2)}) async-start(), calls=%async_computation.3 | async-start | bytes 1179648 | tf_op jit(solution)/shard_map/all_gather | solution.py:16
  16.1 2.1 slice-start
  16.2 2.6 copy-start.26
  16.2 3.6 copy-start.32
  16.2 59.4 %copy-start.23 = (bf16[3,256]{1,0:T(4,128)(2,1)S(1)}, bf16[3,256]{1,0:T(4,128)(2,1)}, u32[]{:S(2)}) copy-start(bf16[3,256]{1,0:T(4,128)(2,1)} %param.32) | copy-start | bytes 4612
  18.2 58.0 %copy-start.17 = (f32[256,1,1,1]{0,2,1,3:T(1,128)}, f32[256,1,1,1]{0,2,1,3:T(1,128)S(1)}, u32[]{:S(2)}) copy-start(f32[256,1,1,1]{0,2,1,3:T(1,128)S(1)} %get-tuple-element.451) | copy-start | bytes 3076
  18.6 57.7 %copy-start.9 = (f32[1,2,128]{2,1,0:T(2,128)}, f32[1,2,128]{2,1,0:T(2,128)S(1)}, u32[]{:S(2)}) copy-start(f32[1,2,128]{2,1,0:T(2,128)S(1)} %reduce_window_sum.17) | copy-start | bytes 3076
  28.8 47.5 %copy-start.6 = (f32[1,2,128]{2,1,0:T(2,128)}, f32[1,2,128]{2,1,0:T(2,128)S(1)}, u32[]{:S(2)}) copy-start(f32[1,2,128]{2,1,0:T(2,128)S(1)} %reduce_window_sum.18) | copy-start | bytes 3076
  32.0 44.2 %copy-start.12 = (f32[1,256]{1,0:T(1,128)}, f32[1,256]{1,0:T(1,128)S(1)}, u32[]{:S(2)}) copy-start(f32[1,256]{1,0:T(1,128)S(1)} %broadcast_add_fusion) | copy-start | bytes 3076
  78.2 68.0 %copy-start = (bf16[256,128]{1,0:T(8,128)(2,1)}, bf16[256,128]{1,0:T(8,128)(2,1)S(1)}, u32[]{:S(2)}) copy-start(bf16[256,128]{1,0:T(8,128)(2,1)S(1)} %convolution_convert_fusion.5) | copy-start | bytes 196612
  147.2 228.0 %all-gather.23.cloned.1.call-start = ((), (), s32[]{:S(2)}) async-start(), calls=%async_computation.4 | async-start | bytes 1179648 | tf_op jit(solution)/shard_map/all_gather | solution.py:16
  245.9 5.4 %collective-permute-start = (bf16[1,256]{0,1:T(8,128)(2,1)S(1)}, bf16[1,256]{0,1:T(8,128)(2,1)S(1)}, u32[]{:S(2)}, u32[]{:S(2)}) collective-permute-start(bf16[1,256]{0,1:T(8,128)(2,1)S(1)} %get-tuple-element.447), channel_id=1, source_target_pairs={{0,4},{4,8},{8,12},{12,16},{16,20},{20,24},{24,28},{1,5},{5,9},{9,... | collective-permute-start | bytes 1544 | tf_op jit(solution)/shard_map/ppermute | solution.py:38
  248.4 7.5 %collective-permute-start.1 = (bf16[1,256]{0,1:T(8,128)(2,1)S(1)}, bf16[1,256]{0,1:T(8,128)(2,1)}, u32[]{:S(2)}, u32[]{:S(2)}) collective-permute-start(bf16[1,256]{0,1:T(8,128)(2,1)S(1)} %get-tuple-element.448), channel_id=1, source_target_pairs={{4,0},{8,4},{12,8},{16,12},{20,16},{24,20},{28,24},{5,1},{9,5},{13... | collective-permute-start | bytes 1544 | tf_op jit(solution)/shard_map/ppermute | solution.py:39
  251.1 173.7 %all-gather.31.cloned.1.call-start = ((), (), s32[]{:S(2)}) async-start(), calls=%async_computation.8 | async-start | bytes 1310720 | tf_op jit(solution)/shard_map/all_gather | solution.py:249
  251.3 0.6 copy-start.8
  293.1 41.0 %copy-start.15 = (f32[1,128]{1,0:T(1,128)S(1)}, f32[1,128]{1,0:T(1,128)}, u32[]{:S(2)}) copy-start(f32[1,128]{1,0:T(1,128)} %custom-call.1) | copy-start | bytes 1540
  293.1 41.0 %copy-start.21 = (f32[8]{0:T(128)S(1)}, f32[8]{0:T(128)}, u32[]{:S(2)}) copy-start(f32[8]{0:T(128)} %get-tuple-element.421) | copy-start | bytes 100
  293.1 41.0 %copy-start.22 = (f32[8]{0:T(128)S(1)}, f32[8]{0:T(128)}, u32[]{:S(2)}) copy-start(f32[8]{0:T(128)} %get-tuple-element.422) | copy-start | bytes 100
  334.1 42.5 %copy-start.14 = (f32[1,128]{1,0:T(1,128)S(1)}, f32[1,128]{1,0:T(1,128)}, u32[]{:S(2)}) copy-start(f32[1,128]{1,0:T(1,128)} %custom-call.3) | copy-start | bytes 1540
  334.1 42.5 %copy-start.19 = (f32[8]{0:T(128)S(1)}, f32[8]{0:T(128)}, u32[]{:S(2)}) copy-start(f32[8]{0:T(128)} %reverse.17) | copy-start | bytes 100
  334.1 42.5 %copy-start.20 = (f32[8]{0:T(128)S(1)}, f32[8]{0:T(128)}, u32[]{:S(2)}) copy-start(f32[8]{0:T(128)} %reverse.18) | copy-start | bytes 100
  363.5 40.6 %copy-start.30 = (f32[1,1,128]{2,1,0:T(1,128)S(1)}, f32[1,1,128]{2,1,0:T(1,128)}, u32[]{:S(2)}) copy-start(f32[1,1,128]{2,1,0:T(1,128)} %get-tuple-element.432) | copy-start | bytes 1540
  363.5 41.0 %copy-start.7 = (f32[1,2,128]{2,1,0:T(2,128)S(1)}, f32[1,2,128]{2,1,0:T(2,128)}, u32[]{:S(2)}) copy-start(f32[1,2,128]{2,1,0:T(2,128)} %copy-done.6) | copy-start | bytes 3076
  363.5 41.0 %copy-start.10 = (f32[1,2,128]{2,1,0:T(2,128)S(1)}, f32[1,2,128]{2,1,0:T(2,128)}, u32[]{:S(2)}) copy-start(f32[1,2,128]{2,1,0:T(2,128)} %copy-done.9) | copy-start | bytes 3076
  363.5 41.0 %copy-start.24 = (f32[2,128]{1,0:T(2,128)S(1)}, f32[2,128]{1,0:T(2,128)}, u32[]{:S(2)}) copy-start(f32[2,128]{1,0:T(2,128)} %get-tuple-element.383) | copy-start | bytes 3076
  363.5 41.0 %copy-start.25 = (f32[2,128]{1,0:T(2,128)S(1)}, f32[2,128]{1,0:T(2,128)}, u32[]{:S(2)}) copy-start(f32[2,128]{1,0:T(2,128)} %get-tuple-element.384) | copy-start | bytes 3076
  363.5 41.1 %copy-start.13 = (f32[1,256]{1,0:T(1,128)S(1)}, f32[1,256]{1,0:T(1,128)}, u32[]{:S(2)}) copy-start(f32[1,256]{1,0:T(1,128)} %copy-done.12) | copy-start | bytes 3076
  376.5 29.0 %copy-start.5 = (f32[1,1,256,128]{3,2,1,0:T(8,128)S(1)}, f32[1,1,256,128]{3,2,1,0:T(8,128)}, u32[]{:S(2)}) copy-start(f32[1,1,256,128]{3,2,1,0:T(8,128)} %get-tuple-element.434) | copy-start | bytes 393220
  400.0 6.6 %copy-start.29 = (f32[1,1,128]{2,1,0:T(1,128)S(1)}, f32[1,1,128]{2,1,0:T(1,128)}, u32[]{:S(2)}) copy-start(f32[1,1,128]{2,1,0:T(1,128)} %get-tuple-element.440) | copy-start | bytes 1540
  400.0 6.7 %copy-start.3 = (f32[256,128]{1,0:T(8,128)S(1)}, f32[256,128]{1,0:T(8,128)}, u32[]{:S(2)}) copy-start(f32[256,128]{1,0:T(8,128)} %get-tuple-element.467) | copy-start | bytes 393220
  400.0 7.0 %copy-start.1 = (bf16[256,128]{1,0:T(8,128)(2,1)S(1)}, bf16[256,128]{1,0:T(8,128)(2,1)}, u32[]{:S(2)}) copy-start(bf16[256,128]{1,0:T(8,128)(2,1)} %copy-done) | copy-start | bytes 196612
  400.0 7.0 %copy-start.18 = (f32[256,1,1,1]{0,2,1,3:T(1,128)S(1)}, f32[256,1,1,1]{0,2,1,3:T(1,128)}, u32[]{:S(2)}) copy-start(f32[256,1,1,1]{0,2,1,3:T(1,128)} %copy-done.17) | copy-start | bytes 3076
  405.0 2.7 copy-start.4
  406.2 2.2 copy-start.31
  406.5 2.0 copy-start.2
  409.3 90.4 %all-gather.33.cloned.1.call-start = ((), (), s32[]{:S(2)}) async-start(), calls=%async_computation.9 | async-start | bytes 4718592 | tf_op jit(solution)/shard_map/all_gather | solution.py:250
Sparse Core Ops, SparseCore 0:
  9.5 43.1 all-gather.16
  54.8 38.9 all-gather.14
  95.9 47.7 all-gather.18
  145.7 47.8 all-gather.26
  195.6 47.5 all-gather.28
  245.2 47.7 all-gather.24
  295.2 38.7 all-gather.20
  336.2 39.0 all-gather.22
  409.4 15.3 all-gather.30
  426.8 72.7 all-gather.32
where the time goes:
time: 513 us; the launch traced here: 511 us
  waiting for transfers between devices  302 us (59%)
  blocking collectives  59.1 us (12%)
  other arithmetic  48.9 us (10%)
  loops' own time  27.5 us (5%)
  matrix products  24.6 us (5%)
  local copies, waits for them, and re-layouts  22.3 us (4%)
  between operations  22.1 us (4%)
    all_gather x1, waiting for transfers between devices, body(): out_whole = lax.all_gather(w_out, 'sp', axis=0, tiled=True)  74.8 us
    all_gather x2, waiting for transfers between devices, carried_in(): pieces = jax.tree.map(lambda part: lax.all_gather(part, axis), value)  49.4 us
    all_gather x1, waiting for transfers between devices, body(): lax.all_gather(w_value, 'sp', axis=0, tiled=True)  47.4 us
    all_gather x1, waiting for transfers between devices, body(): lax.all_gather(w_conv_in, 'sp', axis=0, tiled=True)  47.1 us
    all_gather x1, waiting for transfers between devices, body(): lax.all_gather(w_conv_b, 'sp', axis=0, tiled=True)  36.2 us
    all_gather x2, blocking collectives, carried_in(): pieces = jax.tree.map(lambda part: lax.all_gather(part, axis), value)  35.4 us
    another operation x2, loops' own time, carried_in(): return lax.fori_loop(0, count - 1, lap, subtotal)  27.5 us
    unnamed x1, blocking collectives  23.7 us
  transfers between devices with their start and end apart: 12, of which 10 were waited for; matrix products, arithmetic and copies ran while one was open for 14% of the time, Pallas kernels for 0%

commit v1 on v0

--- a/solution.py
+++ b/solution.py
@@ -2,6 +2,7 @@
 import jax.numpy as jnp
 from jax import lax
 from jax.sharding import PartitionSpec as P
+from jax.lax import axis_index, axis_size, ppermute
 
 DQK = 128
 DV = 256
@@ -247,7 +248,22 @@
     conv_out = conv_branch(gate_outer, gate_inner, conv_input, conv_taps)
     joined = jnp.stack([lstm_out, conv_out], axis=2).reshape(length, -1)
     joined_all = lax.all_gather(joined, "tp", axis=1, tiled=True)
-    out_whole = lax.all_gather(w_out, "sp", axis=0, tiled=True)
+
+    def page_guide(shard_in, named_axis):
+        parts_n = axis_size(named_axis)
+        runs = []
+        for dev_j in tuple(range(parts_n)):
+            runs.append((dev_j, (dev_j + 1) % parts_n))
+        base_arr = [None] * parts_n
+        base_arr[parts_n - 1] = shard_in
+        for d in range(parts_n - 2, -1, -1):
+            base_arr[d] = ppermute(base_arr[d + 1], axis_name=named_axis, perm=runs)
+        odd = jnp.concatenate(base_arr, axis=0)
+        block_out = (axis_index(named_axis) + 1) * shard_in.shape[0]
+        local_out = jnp.roll(odd, block_out, 0)
+        return local_out
+
+    out_whole = page_guide(w_out, "sp")
     return jnp.dot(joined_all, out_whole, preferred_element_type=jnp.float32).astype(jnp.bfloat16)
 
 

time: 513 us -> 482 us (0.940)
  waiting for transfers between devices: 302 us -> 215 us
  local copies, waits for them, and re-layouts: 22.3 us -> 56.1 us
  starting transfers between devices: 4.32 us -> 12.1 us
  other arithmetic: 48.9 us -> 55.9 us
    all_gather x1 -> x0, waiting for transfers between devices: 74.8 us -> none  [body(): out_whole = lax.all_gather(w_out, 'sp', axis=0, tiled=True)]
    ppermute x0 -> x7, waiting for transfers between devices: none -> 50.7 us  [page_guide(): base_arr[d] = ppermute(base_arr[d + 1], axis_name=named_axis, perm=runs)]
    unnamed x75 -> x78, local copies, waits for them, and re-layouts: 5.29 us -> 29.7 us
    all_gather x1, waiting for transfers between devices: 47.4 us -> 29.2 us  [body(): lax.all_gather(w_value, 'sp', axis=0, tiled=True)]
    all_gather x1, waiting for transfers between devices: 15.1 us -> 0.01 us  [body(): lax.all_gather(w_query, 'sp', axis=0, tiled=True)]
    all_gather x1, waiting for transfers between devices: 15 us -> 0.01 us  [body(): joined_all = lax.all_gather(joined, 'tp', axis=1, tiled=True)]
    all_gather x2, waiting for transfers between devices: 49.4 us -> 40.2 us  [carried_in(): pieces = jax.tree.map(lambda part: lax.all_gather(part, axis), value)]
    ppermute x0 -> x7, starting transfers between devices: none -> 7.28 us  [page_guide(): base_arr[d] = ppermute(base_arr[d + 1], axis_name=named_axis, perm=runs)]
  transfers between devices with their start and end apart: 12 -> 18, of which waited for: 10 -> 9; matrix products, arithmetic and copies ran while one was open for 14% -> 24% of each run, Pallas kernels for 0% -> 0%
where the time goes in v1:
time: 482 us; the launch traced here: 479 us
  waiting for transfers between devices  215 us (45%)
  blocking collectives  62.3 us (13%)
  local copies, waits for them, and re-layouts  56.1 us (12%)
  other arithmetic  55.9 us (12%)
  loops' own time  28.9 us (6%)
  matrix products  27.1 us (6%)
  between operations  21.7 us (5%)
  starting transfers between devices  12.1 us (3%)
    all_gather x1, waiting for transfers between devices, body(): lax.all_gather(w_conv_in, 'sp', axis=0, tiled=True)  52.9 us
    ppermute x7, waiting for transfers between devices, page_guide(): base_arr[d] = ppermute(base_arr[d + 1], axis_name=named_axis, perm=runs)  50.7 us
    all_gather x2, waiting for transfers between devices, carried_in(): pieces = jax.tree.map(lambda part: lax.all_gather(part, axis), value)  40.2 us
    all_gather x2, blocking collectives, carried_in(): pieces = jax.tree.map(lambda part: lax.all_gather(part, axis), value)  35.3 us
    all_gather x1, waiting for transfers between devices, body(): lax.all_gather(w_conv_b, 'sp', axis=0, tiled=True)  32.1 us
    unnamed x78, local copies, waits for them, and re-layouts  29.7 us
    all_gather x1, waiting for transfers between devices, body(): lax.all_gather(w_value, 'sp', axis=0, tiled=True)  29.2 us
    another operation x2, loops' own time, carried_in(): return lax.fori_loop(0, count - 1, lap, subtotal)  28.9 us
  transfers between devices with their start and end apart: 18, of which 9 were waited for; matrix products, arithmetic and copies ran while one was open for 24% of the time, Pallas kernels for 0%

profile of v1, /device:TPU:0, one launch (start us, length us, event | category | flops | bytes accessed | tf_op | source)
XLA Modules:
  0.0 479.5 jit_solution(12625044954124433917)
XLA Ops:
  9.9 3.0 collective-permute-start.2
  13.1 2.1 fusion.8
  16.6 1.4 fusion.87
  18.7 2.3 fusion.10
  26.0 1.9 fusion.71
  28.7 3.7 fusion.90
  34.5 1.9 fusion.70
  37.0 1.6 collective-permute-start.3
  39.3 3.6 fusion.93
  44.2 27.0 %all-reduce.8 = (f32[8]{0:T(128)}, f32[8]{0:T(128)}, f32[8]{0:T(128)S(1)}, f32[8]{0:T(128)S(1)}) all-reduce(f32[8]{0:T(128)S(1)} %fusion.71, f32[8]{0:T(128)S(1)} %dynamic-update-slice.1, f32[8]{0:T(128)S(1)} %fusion.70, f32[8]{0:T(128)S(1)} %dynamic-update-slice.3), channel_id=2, replica_groups=mesh['sp'=8,'tp'=4] {'sp'}, use_global_device_ids=true, to_apply=%add.4 | all-reduce | flops 32 | bytes 256
  71.4 1.8 fusion.91
  77.2 1.8 fusion.94
  84.3 2.3 collective-permute-start.4
  88.1 20.0 %collective-permute-done.4 = bf16[256,1024]{1,0:T(8,128)(2,1)} collective-permute-done((bf16[256,1024]{1,0:T(8,128)(2,1)}, bf16[256,1024]{1,0:T(8,128)(2,1)}, u32[]{:S(2)}, u32[]{:S(2)}) %collective-permute-start.4) | collective-permute-done | bytes 524320 | tf_op jit(solution)/shard_map/ppermute | solution.py:260
  108.2 1.9 convolution_convert_fusion.4
  110.4 14.0 %collective-permute-done.5 = bf16[256,1024]{1,0:T(8,128)(2,1)} collective-permute-done((bf16[256,1024]{1,0:T(8,128)(2,1)}, bf16[256,1024]{1,0:T(8,128)(2,1)}, u32[]{:S(2)}, u32[]{:S(2)}) %collective-permute-start.5) | collective-permute-done | bytes 524320 | tf_op jit(solution)/shard_map/ppermute | solution.py:260
  125.2 2.7 broadcast_multiply_fusion.1
  127.8 16.7 %collective-permute-done.6 = bf16[256,1024]{1,0:T(8,128)(2,1)} collective-permute-done((bf16[256,1024]{1,0:T(8,128)(2,1)}, bf16[256,1024]{1,0:T(8,128)(2,1)}, u32[]{:S(2)}, u32[]{:S(2)}) %collective-permute-start.6) | collective-permute-done | bytes 524320 | tf_op jit(solution)/shard_map/ppermute | solution.py:260
  144.5 29.2 %all-gather.18.cloned.1.call-done = bf16[4096,256]{1,0:T(8,128)(2,1)} async-done(((bf16[512,256]{1,0:T(8,128)(2,1)}), bf16[4096,256]{1,0:T(8,128)(2,1)}) %all-gather.18.cloned.1.call-update) | async-done | bytes 2097168 | tf_op jit(solution)/shard_map/all_gather | solution.py:229
  173.7 2.3 fusion.89
  180.3 17.1 %all_gather.75 = f32[8,1,128]{2,1,0:T(1,128)S(1)} all-gather(f32[1,1,128]{2,1,0:T(1,128)S(1)} %get-tuple-element.431), channel_id=1, replica_groups=mesh['sp'=8,'tp'=4] {'sp'}, dimensions={0}, use_global_device_ids=true | all-gather | bytes 4608 | tf_op jit(solution)/shard_map/all_gather | solution.py:17
  199.4 18.2 %all_gather.69 = f32[8,1,128]{2,1,0:T(1,128)} all-gather(f32[1,1,128]{2,1,0:T(1,128)S(1)} %get-tuple-element.439), channel_id=1, replica_groups=mesh['sp'=8,'tp'=4] {'sp'}, dimensions={0}, use_global_device_ids=true | all-gather | bytes 4608 | tf_op jit(solution)/shard_map/all_gather | solution.py:17
  218.6 6.9 %all-gather.26.cloned.1.call-done = bf16[4096,256]{1,0:T(8,128)(2,1)} async-done(((bf16[512,256]{1,0:T(8,128)(2,1)}), bf16[4096,256]{1,0:T(8,128)(2,1)}) %all-gather.26.cloned.1.call-update) | async-done | bytes 2097168 | tf_op jit(solution)/shard_map/all_gather | solution.py:231
  225.5 2.5 fusion.25
  228.0 52.9 %all-gather.28.cloned.1.call-done = bf16[4096,256]{1,0:T(8,128)(2,1)} async-done(((bf16[512,256]{1,0:T(8,128)(2,1)}), bf16[4096,256]{1,0:T(8,128)(2,1)}) %all-gather.28.cloned.1.call-update) | async-done | bytes 2097168 | tf_op jit(solution)/shard_map/all_gather | solution.py:232
  280.9 2.5 fusion.24
  284.2 3.1 collective-permute-start
  291.0 1.9 constant_dynamic-update-slice_fusion.15
  292.9 1.9 constant_dynamic-update-slice_fusion.14
  294.8 1.9 constant_dynamic-update-slice_fusion.13
  296.7 1.8 maximum_convert_fusion
  298.5 32.1 %all-gather.24.cloned.1.call-done = bf16[4096,256]{1,0:T(8,128)(2,1)} async-done(((bf16[512,256]{1,0:T(8,128)(2,1)}), bf16[4096,256]{1,0:T(8,128)(2,1)}) %all-gather.24.cloned.1.call-update) | async-done | bytes 2097168 | tf_op jit(solution)/shard_map/all_gather | solution.py:230
  330.6 3.5 fusion.29
  334.1 37.4 %all-gather.20.cloned.1.call-done = f32[8,1,256,128]{3,2,1,0:T(8,128)} async-done(((f32[1,1,256,128]{3,2,1,0:T(8,128)}), f32[8,1,256,128]{3,2,1,0:T(8,128)}) %all-gather.20.cloned.1.call-update) | async-done | bytes 1048592 | tf_op jit(solution)/shard_map/all_gather | solution.py:17
  371.5 38.3 %while.36 = (s32[]{:T(128)}, f32[1,256,128]{2,1,0:T(8,128)S(1)}, f32[1,128]{1,0:T(1,128)}, f32[1]{0:T(128)}, s32[]{:T(128)}, /*index=5*/f32[8,1]{0,1:T(1,128)}, ...) while((s32[]{:T(128)}, f32[1,256,128]{2,1,0:T(8,128)S(1)}, ...), condition=%wide.region_4.5_spmd.clone, body=%wide.region_3.4_spmd.clone.sunk | while | flops 164489 | bytes 395012 | solution.py:29
  409.9 2.8 all-gather.22.cloned.1.call-done
  414.0 23.5 %while.37 = (s32[]{:T(128)}, f32[1,256,128]{2,1,0:T(8,128)S(1)}, f32[1,128]{1,0:T(1,128)S(1)}, f32[1]{0:T(128)}, s32[]{:T(128)}, /*index=5*/f32[8,1]{0,1:T(1,128...) while((s32[]{:T(128)}, f32[1,256,128]{2,1,0:T(8,128)S(1)}, ...), condition=%wide.region_10.11_spmd.clone, body=%wide.region_9.10_spmd.clone.sunk | while | flops 164489 | bytes 395012 | solution.py:29
  437.5 1.4 subtract_exponential_fusion.7
  448.0 1.9 constant_dynamic-update-slice_fusion.12
  449.9 1.9 constant_dynamic-update-slice_fusion.11
  451.8 1.9 constant_dynamic-update-slice_fusion.10
  455.3 1.9 constant_dynamic-update-slice_fusion.7
  457.2 1.9 constant_dynamic-update-slice_fusion.6
  459.1 1.9 constant_dynamic-update-slice_fusion.5
  461.0 1.9 constant_dynamic-update-slice_fusion.4
  462.8 1.9 constant_dynamic-update-slice_fusion.3
  464.7 1.9 constant_dynamic-update-slice_fusion.2
  468.4 4.6 fusion.15
  (212 shorter events, 78.5 us)
Async XLA Ops:
  6.5 101.6 %all-gather.16.cloned.1.call-start = ((), (), s32[]{:S(2)}) async-start(), calls=%async_computation.1 | async-start | bytes 1179648 | tf_op jit(solution)/shard_map/all_gather | solution.py:228
  7.3 117.9 %all-gather.14.cloned.1.call-start = ((), (), s32[]{:S(2)}) async-start(), calls=%async_computation | async-start | bytes 1179648 | tf_op jit(solution)/shard_map/all_gather | solution.py:227
  8.0 165.7 %all-gather.18.cloned.1.call-start = ((), (), s32[]{:S(2)}) async-start(), calls=%async_computation.2 | async-start | bytes 2359296 | tf_op jit(solution)/shard_map/all_gather | solution.py:229
  8.7 216.7 %all-gather.26.cloned.1.call-start = ((), (), s32[]{:S(2)}) async-start(), calls=%async_computation.6 | async-start | bytes 2359296 | tf_op jit(solution)/shard_map/all_gather | solution.py:231
  9.3 271.6 %all-gather.28.cloned.1.call-start = ((), (), s32[]{:S(2)}) async-start(), calls=%async_computation.7 | async-start | bytes 2359296 | tf_op jit(solution)/shard_map/all_gather | solution.py:232
  9.9 320.7 %all-gather.24.cloned.1.call-start = ((), (), s32[]{:S(2)}) async-start(), calls=%async_computation.5 | async-start | bytes 2359296 | tf_op jit(solution)/shard_map/all_gather | solution.py:230
  9.9 27.0 %collective-permute-start.2 = (bf16[256,1024]{1,0:T(8,128)(2,1)}, bf16[256,1024]{1,0:T(8,128)(2,1)S(1)}, u32[]{:S(2)}, u32[]{:S(2)}) collective-permute-start(bf16[256,1024]{1,0:T(8,128)(2,1)} %param.33), channel_id=1, source_target_pairs={{0,4},{4,8},{8,12},{12,16},{16,20},{20,24},{24,28},{28,0},{1,5},{5... | collective-permute-start | bytes 1572872 | tf_op jit(solution)/shard_map/ppermute | solution.py:260
  13.0 358.5 %all-gather.20.cloned.1.call-start = ((), (), s32[]{:S(2)}) async-start(), calls=%async_computation.3 | async-start | bytes 1179648 | tf_op jit(solution)/shard_map/all_gather | solution.py:17
  13.1 8.6 %copy-start.24 = (f32[2,256,1]{1,2,0:T(1,128)S(1)}, f32[2,256,1]{1,2,0:T(1,128)}, u32[]{:S(2)}) copy-start(f32[2,256,1]{1,2,0:T(1,128)} %param.27) | copy-start | bytes 6148
  13.1 10.7 %slice-start = ((f32[2,256,1]{1,2,0:T(1,128)}), f32[1,256,1]{1,2,0:T(1,128)S(1)}, s32[]{:S(2)}) async-start(f32[2,256,1]{1,2,0:T(1,128)} %param.27), calls=%async_computation.9 | async-start | bytes 2048 | tf_op jit(solution)/shard_map/slice | solution.py:165
  13.1 11.5 %copy-start.26 = (u32[32]{0:T(128)S(1)}, u32[32]{0:T(128)}, u32[]{:S(2)}) copy-start(u32[32]{0:T(128)} %constant.181) | copy-start | bytes 388
  13.1 74.3 %copy-start.21 = (bf16[3,256]{1,0:T(4,128)(2,1)S(1)}, bf16[3,256]{1,0:T(4,128)(2,1)}, u32[]{:S(2)}) copy-start(bf16[3,256]{1,0:T(4,128)(2,1)} %param.32) | copy-start | bytes 4612
  23.8 84.3 %copy-start.16 = (f32[256,1,1,1]{0,2,1,3:T(1,128)}, f32[256,1,1,1]{0,2,1,3:T(1,128)S(1)}, u32[]{:S(2)}) copy-start(f32[256,1,1,1]{0,2,1,3:T(1,128)S(1)} %get-tuple-element.451) | copy-start | bytes 3076
  24.2 83.9 %copy-start.10 = (f32[1,2,128]{2,1,0:T(2,128)}, f32[1,2,128]{2,1,0:T(2,128)S(1)}, u32[]{:S(2)}) copy-start(f32[1,2,128]{2,1,0:T(2,128)S(1)} %reduce_window_sum.17) | copy-start | bytes 3076
  25.4 82.7 %copy-start.8 = (f32[1,2,128]{2,1,0:T(2,128)}, f32[1,2,128]{2,1,0:T(2,128)S(1)}, u32[]{:S(2)}) copy-start(f32[1,2,128]{2,1,0:T(2,128)S(1)} %reduce_window_sum.18) | copy-start | bytes 3076
  36.9 71.2 %copy-start.12 = (f32[1,256]{1,0:T(1,128)}, f32[1,256]{1,0:T(1,128)S(1)}, u32[]{:S(2)}) copy-start(f32[1,256]{1,0:T(1,128)S(1)} %broadcast_add_fusion) | copy-start | bytes 3076
  37.0 47.3 %collective-permute-start.3 = (bf16[256,1024]{1,0:T(8,128)(2,1)S(1)}, bf16[256,1024]{1,0:T(8,128)(2,1)}, u32[]{:S(2)}, u32[]{:S(2)}) collective-permute-start(bf16[256,1024]{1,0:T(8,128)(2,1)S(1)} %collective-permute-done.2), channel_id=1, source_target_pairs={{0,4},{4,8},{8,12},{12,16},{16,20},{20,24},{24,28},{28,0},{1,5},{5... | collective-permute-start | bytes 1572872 | tf_op jit(solution)/shard_map/ppermute | solution.py:260
  84.3 23.8 %collective-permute-start.4 = (bf16[256,1024]{1,0:T(8,128)(2,1)}, bf16[256,1024]{1,0:T(8,128)(2,1)}, u32[]{:S(2)}, u32[]{:S(2)}) collective-permute-start(bf16[256,1024]{1,0:T(8,128)(2,1)} %collective-permute-done.3), channel_id=1, source_target_pairs={{0,4},{4,8},{8,12},{12,16},{16,20},{20,24},{24,28},{28,0},{1,5},{5... | collective-permute-start | bytes 1572872 | tf_op jit(solution)/shard_map/ppermute | solution.py:260
  87.5 88.5 %copy-start.20 = (f32[2,128]{1,0:T(2,128)}, f32[2,128]{1,0:T(2,128)S(1)}, u32[]{:S(2)}) copy-start(f32[2,128]{1,0:T(2,128)S(1)} %subtract_exponential_fusion.1) | copy-start | bytes 3076
  108.1 16.3 %collective-permute-start.5 = (bf16[256,1024]{1,0:T(8,128)(2,1)}, bf16[256,1024]{1,0:T(8,128)(2,1)}, u32[]{:S(2)}, u32[]{:S(2)}) collective-permute-start(bf16[256,1024]{1,0:T(8,128)(2,1)} %collective-permute-done.4), channel_id=1, source_target_pairs={{0,4},{4,8},{8,12},{12,16},{16,20},{20,24},{24,28},{28,0},{1,5},{5... | collective-permute-start | bytes 1572872 | tf_op jit(solution)/shard_map/ppermute | solution.py:260
  110.1 66.8 %copy-start.2 = (bf16[256,128]{1,0:T(8,128)(2,1)}, bf16[256,128]{1,0:T(8,128)(2,1)S(1)}, u32[]{:S(2)}) copy-start(bf16[256,128]{1,0:T(8,128)(2,1)S(1)} %convolution_convert_fusion.4) | copy-start | bytes 196612
  124.4 20.1 %collective-permute-start.6 = (bf16[256,1024]{1,0:T(8,128)(2,1)}, bf16[256,1024]{1,0:T(8,128)(2,1)}, u32[]{:S(2)}, u32[]{:S(2)}) collective-permute-start(bf16[256,1024]{1,0:T(8,128)(2,1)} %collective-permute-done.5), channel_id=1, source_target_pairs={{0,4},{4,8},{8,12},{12,16},{16,20},{20,24},{24,28},{28,0},{1,5},{5... | collective-permute-start | bytes 1572872 | tf_op jit(solution)/shard_map/ppermute | solution.py:260
  144.5 73.7 %collective-permute-start.7 = (bf16[256,1024]{1,0:T(8,128)(2,1)}, bf16[256,1024]{1,0:T(8,128)(2,1)}, u32[]{:S(2)}, u32[]{:S(2)}) collective-permute-start(bf16[256,1024]{1,0:T(8,128)(2,1)} %collective-permute-done.6), channel_id=1, source_target_pairs={{0,4},{4,8},{8,12},{12,16},{16,20},{20,24},{24,28},{28,0},{1,5},{5... | collective-permute-start | bytes 1572872 | tf_op jit(solution)/shard_map/ppermute | solution.py:260
  178.8 233.9 %all-gather.22.cloned.1.call-start = ((), (), s32[]{:S(2)}) async-start(), calls=%async_computation.4 | async-start | bytes 1179648 | tf_op jit(solution)/shard_map/all_gather | solution.py:17
  218.2 72.8 %collective-permute-start.8 = (bf16[256,1024]{1,0:T(8,128)(2,1)}, bf16[256,1024]{1,0:T(8,128)(2,1)}, u32[]{:S(2)}, u32[]{:S(2)}) collective-permute-start(bf16[256,1024]{1,0:T(8,128)(2,1)} %collective-permute-done.7), channel_id=1, source_target_pairs={{0,4},{4,8},{8,12},{12,16},{16,20},{20,24},{24,28},{28,0},{1,5},{5... | collective-permute-start | bytes 1572872 | tf_op jit(solution)/shard_map/ppermute | solution.py:260
  284.2 12.5 %collective-permute-start = (bf16[1,256]{0,1:T(8,128)(2,1)}, bf16[1,256]{0,1:T(8,128)(2,1)}, u32[]{:S(2)}, u32[]{:S(2)}) collective-permute-start(bf16[1,256]{0,1:T(8,128)(2,1)} %get-tuple-element.447), channel_id=1, source_target_pairs={{0,4},{4,8},{8,12},{12,16},{16,20},{20,24},{24,28},{1,5},{5,9},{9,... | collective-permute-start | bytes 1544 | tf_op jit(solution)/shard_map/ppermute | solution.py:39
  287.3 9.4 %collective-permute-start.1 = (bf16[1,256]{0,1:T(8,128)(2,1)}, bf16[1,256]{0,1:T(8,128)(2,1)}, u32[]{:S(2)}, u32[]{:S(2)}) collective-permute-start(bf16[1,256]{0,1:T(8,128)(2,1)} %get-tuple-element.448), channel_id=1, source_target_pairs={{4,0},{8,4},{12,8},{16,12},{20,16},{24,20},{28,24},{5,1},{9,5},{13... | collective-permute-start | bytes 1544 | tf_op jit(solution)/shard_map/ppermute | solution.py:40
  290.8 177.6 %all-gather.30.cloned.1.call-start = ((), (), s32[]{:S(2)}) async-start(), calls=%async_computation.8 | async-start | bytes 1310720 | tf_op jit(solution)/shard_map/all_gather | solution.py:250
  334.1 79.9 %copy-start.14 = (f32[1,128]{1,0:T(1,128)S(1)}, f32[1,128]{1,0:T(1,128)}, u32[]{:S(2)}) copy-start(f32[1,128]{1,0:T(1,128)} %custom-call.3) | copy-start | bytes 1540
  334.1 80.0 %copy-start.18 = (f32[8]{0:T(128)S(1)}, f32[8]{0:T(128)}, u32[]{:S(2)}) copy-start(f32[8]{0:T(128)} %reverse.17) | copy-start | bytes 100
  334.1 80.0 %copy-start.19 = (f32[8]{0:T(128)S(1)}, f32[8]{0:T(128)}, u32[]{:S(2)}) copy-start(f32[8]{0:T(128)} %reverse.18) | copy-start | bytes 100
  334.1 107.5 %copy-start.25 = (f32[1,1,128]{2,1,0:T(1,128)S(1)}, f32[1,1,128]{2,1,0:T(1,128)}, u32[]{:S(2)}) copy-start(f32[1,1,128]{2,1,0:T(1,128)} %get-tuple-element.432) | copy-start | bytes 1540
  334.1 107.5 %copy-start.1 = (f32[256,128]{1,0:T(8,128)S(1)}, f32[256,128]{1,0:T(8,128)}, u32[]{:S(2)}) copy-start(f32[256,128]{1,0:T(8,128)} %broadcast_multiply_fusion) | copy-start | bytes 393220
  334.1 107.8 %copy-start.9 = (f32[1,2,128]{2,1,0:T(2,128)S(1)}, f32[1,2,128]{2,1,0:T(2,128)}, u32[]{:S(2)}) copy-start(f32[1,2,128]{2,1,0:T(2,128)} %copy-done.8) | copy-start | bytes 3076
  334.1 107.8 %copy-start.11 = (f32[1,2,128]{2,1,0:T(2,128)S(1)}, f32[1,2,128]{2,1,0:T(2,128)}, u32[]{:S(2)}) copy-start(f32[1,2,128]{2,1,0:T(2,128)} %copy-done.10) | copy-start | bytes 3076
  334.1 107.8 %copy-start.22 = (f32[2,128]{1,0:T(2,128)S(1)}, f32[2,128]{1,0:T(2,128)}, u32[]{:S(2)}) copy-start(f32[2,128]{1,0:T(2,128)} %get-tuple-element.383) | copy-start | bytes 3076
  334.1 107.8 %copy-start.23 = (f32[2,128]{1,0:T(2,128)S(1)}, f32[2,128]{1,0:T(2,128)}, u32[]{:S(2)}) copy-start(f32[2,128]{1,0:T(2,128)} %get-tuple-element.384) | copy-start | bytes 3076
  334.1 107.9 %copy-start.13 = (f32[1,256]{1,0:T(1,128)S(1)}, f32[1,256]{1,0:T(1,128)}, u32[]{:S(2)}) copy-start(f32[1,256]{1,0:T(1,128)} %copy-done.12) | copy-start | bytes 3076
  334.1 108.8 %copy-start.7 = (f32[1,1,256,128]{3,2,1,0:T(8,128)S(1)}, f32[1,1,256,128]{3,2,1,0:T(8,128)}, u32[]{:S(2)}) copy-start(f32[1,1,256,128]{3,2,1,0:T(8,128)} %get-tuple-element.434) | copy-start | bytes 393220
  409.8 34.1 %copy-start.15 = (f32[1,128]{1,0:T(1,128)S(1)}, f32[1,128]{1,0:T(1,128)}, u32[]{:S(2)}) copy-start(f32[1,128]{1,0:T(1,128)} %get-tuple-element.319) | copy-start | bytes 1540
  409.9 34.9 %copy-start.5 = (f32[256,128]{1,0:T(8,128)S(1)}, f32[256,128]{1,0:T(8,128)}, u32[]{:S(2)}) copy-start(f32[256,128]{1,0:T(8,128)} %get-tuple-element.467) | copy-start | bytes 393220
  409.9 35.2 %copy-start.3 = (bf16[256,128]{1,0:T(8,128)(2,1)S(1)}, bf16[256,128]{1,0:T(8,128)(2,1)}, u32[]{:S(2)}) copy-start(bf16[256,128]{1,0:T(8,128)(2,1)} %copy-done.2) | copy-start | bytes 196612
  409.9 35.2 %copy-start.17 = (f32[256,1,1,1]{0,2,1,3:T(1,128)S(1)}, f32[256,1,1,1]{0,2,1,3:T(1,128)}, u32[]{:S(2)}) copy-start(f32[256,1,1,1]{0,2,1,3:T(1,128)} %copy-done.16) | copy-start | bytes 3076
  409.9 35.9 %copy-start.6 = (f32[1,1,256,128]{3,2,1,0:T(8,128)S(1)}, f32[1,1,256,128]{3,2,1,0:T(8,128)}, u32[]{:S(2)}) copy-start(f32[1,1,256,128]{3,2,1,0:T(8,128)} %get-tuple-element.442) | copy-start | bytes 393220
  437.5 9.8 %copy-start.4 = (bf16[256,1,1,256]{0,3,2,1:T(8,128)(2,1)S(1)}, bf16[256,1,1,256]{0,3,2,1:T(8,128)(2,1)}, u32[]{:S(2)}) copy-start(bf16[256,1,1,256]{0,3,2,1:T(8,128)(2,1)} %fusion.29) | copy-start | bytes 393220
  445.4 9.0 %copy-start = (bf16[256,1024]{1,0:T(8,128)(2,1)S(1)}, bf16[256,1024]{1,0:T(8,128)(2,1)}, u32[]{:S(2)}) copy-start(bf16[256,1024]{1,0:T(8,128)(2,1)} %param.33) | copy-start | bytes 1572868
Sparse Core Ops, SparseCore 0:
  9.5 50.9 all-gather.15
  62.6 43.5 all-gather.13
  108.3 65.3 all-gather.17
  175.7 49.7 all-gather.25
  227.5 53.4 all-gather.27
  282.9 47.6 all-gather.23
  332.7 38.7 all-gather.19
  373.7 38.9 all-gather.21
  448.1 15.4 all-gather.29
